TPU v7x, 128 devices: a whole 4x4x4 slice. The times are simulated.
128 devices in a mesh: fs: 16 (over z, y), tp: 8 (over x, core).
Axes of the slice: x: 4, y: 4, z: 4, core: 2. Of those that a mesh axis runs over, the one named last changes fastest.
Arguments:
- late_input: bfloat16 [8192, 2048], P(('fs', 'tp')), may hold values from -6 to 6
- early_input: bfloat16 [8192, 2048], P(('fs', 'tp')), may hold values from -6 to 6
- early_grad: bfloat16 [8192, 2048], P(('fs', 'tp')), may hold values from -24 to 24
- pre_gain: float32 [2048], replicated, may hold values from 0.1 to 1.9
- post_gain: float32 [2048], replicated, may hold values from 0.1 to 1.9
- gate_weight: bfloat16 [2048, 4096], P('fs', 'tp'), may hold values from -0.125 to 0.125
- up_weight: bfloat16 [2048, 4096], P('fs', 'tp'), may hold values from -0.125 to 0.125
- down_weight: bfloat16 [2048, 4096], P('fs', 'tp'), may hold values from -0.09375 to 0.09375
- gate_sum: float32 [2048, 4096], P('fs', 'tp'), may hold values from -1.8 to 1.8
- up_sum: float32 [2048, 4096], P('fs', 'tp'), may hold values from -1.8 to 1.8
- down_gradient_sum: float32 [2048, 4096], P('fs', 'tp'), may hold values from -1.8 to 1.8
Outputs:
- late_output: bfloat16 [8192, 2048], P(('fs', 'tp'))
- early_input_grad: bfloat16 [8192, 2048], P(('fs', 'tp'))
- gate_total: float32 [2048, 4096], P('fs', 'tp')
- up_total: float32 [2048, 4096], P('fs', 'tp')
- down_total: float32 [2048, 4096], P('fs', 'tp')
All inputs are finite; a program needn't handle non-finite values.
Results may differ from a plain program's by a relative error of at most 0.013.
Values may be sent and summed in bfloat16 or wider, within the bound.
A program may use at most 128 MiB of HBM per device.

v0:
```python
import math
import jax
import jax.numpy as jnp
from jax import lax
from jax.sharding import PartitionSpec as P

NORM_EPS = 1e-06


def sent_together(arrays, axis, dim, along):
    ends, at = ([], 0)
    for a in arrays[:-1]:
        at += a.shape[along]
        ends.append(at)
    both = jnp.concatenate(arrays, axis=along)
    return tuple(jnp.split(lax.all_gather(both, axis, axis=dim, tiled=True), ends, axis=along))


def sent_to_all(shard, axis):
    peers = lax.axis_size(axis)
    return lax.all_to_all(
        jnp.broadcast_to(shard[None], (peers, *shard.shape)), axis, 0, 0, tiled=True
    )


def in_order(parts, dim):
    parts = jnp.moveaxis(parts, 0, dim)
    dims = parts.shape
    return parts.reshape(*dims[:dim], dims[dim] * dims[dim + 1], *dims[dim + 2 :])


def gather_directly(shard, axis, dim):
    parts = sent_to_all(shard, axis)
    return in_order(parts, dim)


def in_blocks(shard, dim, peers):
    dims = shard.shape
    parts = shard.reshape(*dims[:dim], peers, dims[dim] // peers, *dims[dim + 1 :])
    return jnp.moveaxis(parts, dim, 0)


def summed_on_arrival(shard, axis, dim):
    parts = in_blocks(shard, dim, lax.axis_size(axis))
    arrived = lax.all_to_all(parts, axis, split_axis=0, concat_axis=0, tiled=True)
    return arrived.astype(jnp.float32).sum(axis=0)


def contract_last(first_op, second_op):
    return lax.dot_general(
        first_op, second_op, (((1,), (1,)), ((), ())), preferred_element_type=jnp.float32
    )


def contract_first(first_op, second_op):
    return lax.dot_general(
        first_op, second_op, (((0,), (0,)), ((), ())), preferred_element_type=jnp.float32
    )


def inverse_rms(values):
    return lax.rsqrt(jnp.mean(values * values, axis=-1, keepdims=True) + NORM_EPS)


def per_device(
    late_input,
    early_input,
    early_grad,
    pre_gain,
    post_gain,
    gate_weight,
    up_weight,
    down_weight,
    gate_sum,
    up_sum,
    down_gradient_sum,
):
    tok_rows, model_width = late_input.shape
    group_rows = tok_rows * lax.axis_size("tp")
    grad_scale = 1.0 / math.sqrt(group_rows * lax.axis_size("fs"))
    hidden_width = gate_sum.shape[1]
    input_rows = jnp.stack([late_input, early_input]).astype(jnp.float32)
    input_inverse = inverse_rms(input_rows)
    normed = (input_rows * input_inverse * pre_gain).astype(jnp.bfloat16)
    normed_rows = lax.all_gather(normed, "tp", axis=1, tiled=True)
    gate_all, up_all, down_gradient_rows = sent_together(
        (gate_weight, up_weight, down_weight), "fs", 0, 1
    )
    flat_rows = normed_rows.reshape(2 * group_rows, model_width)
    gate_pre = jnp.dot(flat_rows, gate_all, preferred_element_type=jnp.float32)
    up_pre = jnp.dot(flat_rows, up_all, preferred_element_type=jnp.float32)
    hidden_state = (
        (jax.nn.silu(gate_pre) * up_pre).astype(jnp.bfloat16).reshape(2, group_rows, hidden_width)
    )
    gated_product = jnp.einsum(
        "utx,ix->tui", hidden_state, down_gradient_rows, preferred_element_type=jnp.float32
    )
    mixed_sum = lax.psum_scatter(
        gated_product.reshape(lax.axis_size("tp") * tok_rows, 2 * model_width).astype(jnp.bfloat16),
        "tp",
        scatter_dimension=0,
        tiled=True,
    ).astype(jnp.float32)
    mixed_sum = lax.optimization_barrier(mixed_sum.astype(jnp.bfloat16)).astype(jnp.float32)
    mixed_sum = mixed_sum.reshape(tok_rows, 2, model_width)
    mixed_inverse = inverse_rms(mixed_sum)
    late_output = (input_rows[0] + 0.5 * mixed_sum[:, 0] * mixed_inverse[:, 0] * post_gain).astype(
        jnp.bfloat16
    )
    early_mixed = mixed_sum[:, 1]
    early_inverse_norm = mixed_inverse[:, 1]
    weighted = 0.5 * early_grad.astype(jnp.float32) * post_gain
    mixed_cot = (
        early_inverse_norm * weighted
        - early_mixed
        * early_inverse_norm**3
        * jnp.mean(weighted * early_mixed, axis=-1, keepdims=True)
    ).astype(jnp.bfloat16)
    cot_rows = gather_directly(mixed_cot, "tp", 0)
    early_hidden = hidden_state[1]
    early_normed = normed_rows[1]
    hidden_cot = jnp.dot(cot_rows, down_gradient_rows, preferred_element_type=jnp.float32)
    early_gate = gate_pre[group_rows:]
    early_up = up_pre[group_rows:]
    sigmoid_gate = jax.nn.sigmoid(early_gate)
    gate_cot = (
        hidden_cot * early_up * sigmoid_gate * (1.0 + early_gate * (1.0 - sigmoid_gate))
    ).astype(jnp.bfloat16)
    up_cot = (hidden_cot * early_gate * sigmoid_gate).astype(jnp.bfloat16)
    normed_cot = summed_on_arrival(
        (contract_last(gate_cot, gate_all) + contract_last(up_cot, up_all)).astype(jnp.bfloat16),
        "tp",
        0,
    )
    normed_cot = lax.optimization_barrier(normed_cot.astype(jnp.bfloat16)).astype(jnp.float32)
    weighted_in = normed_cot * pre_gain
    early_values = input_rows[1]
    early_in_inverse = input_inverse[1]
    early_input_grad = (
        early_grad.astype(jnp.float32)
        + early_in_inverse * weighted_in
        - early_values
        * early_in_inverse**3
        * jnp.mean(weighted_in * early_values, axis=-1, keepdims=True)
    ).astype(jnp.bfloat16)
    totals = lax.psum_scatter(
        (
            grad_scale
            * jnp.concatenate(
                [
                    contract_first(early_normed, gate_cot),
                    contract_first(early_normed, up_cot),
                    contract_first(cot_rows, early_hidden),
                ],
                1,
            )
        ).astype(jnp.bfloat16),
        "fs",
        scatter_dimension=0,
        tiled=True,
    ).astype(jnp.float32)
    gate_total = gate_sum + totals[:, :hidden_width]
    up_total = up_sum + totals[:, hidden_width : 2 * hidden_width]
    down_total = down_gradient_sum + totals[:, 2 * hidden_width :]
    return (late_output, early_input_grad, gate_total, up_total, down_total)


def solution(mesh):
    in_specs = (
        P(("fs", "tp"), None),
        P(("fs", "tp"), None),
        P(("fs", "tp"), None),
        P(),
        P(),
        P("fs", "tp"),
        P("fs", "tp"),
        P("fs", "tp"),
        P("fs", "tp"),
        P("fs", "tp"),
        P("fs", "tp"),
    )
    out_specs = (
        P(("fs", "tp"), None),
        P(("fs", "tp"), None),
        P("fs", "tp"),
        P("fs", "tp"),
        P("fs", "tp"),
    )
    return jax.shard_map(
        per_device, mesh=mesh, in_specs=in_specs, out_specs=out_specs, check_vma=False
    )
```

profile of v0, /device:TPU:0, one launch (start us, length us, event | category | flops | bytes accessed | tf_op | source)
XLA Modules:
  0.0 314.3 jit_solution(15130578604359886631)
XLA Ops:
  7.2 1.2 multiply_reduce_fusion.1
  8.4 2.0 multiply_convert_fusion.2
  10.5 0.0 all-gather.3.cloned.1.call-start
  10.5 1.8 pad_maximum_fusion
  12.4 0.0 reduce-scatter.5.cloned.1.call-start
  12.4 32.7 %all-gather.5.cloned.1.call-done = bf16[2,512,2048]{2,1,0:T(8,128)(2,1)} async-done(((bf16[2,64,2048]{2,1,0:T(8,128)(2,1)}), bf16[2,512,2048]{2,1,0:T(8,128)(2,1)}) %all-gather.5.cloned.1.call-update) | async-done | bytes 4194320 | tf_op jit(solution)/shard_map/all_gather | solution.py:85
  45.2 63.5 %all-gather.3.cloned.1.call-done = bf16[2048,1536]{1,0:T(8,128)(2,1)} async-done(((bf16[128,1536]{1,0:T(8,128)(2,1)}), bf16[2048,1536]{1,0:T(8,128)(2,1)}) %all-gather.3.cloned.1.call-update) | async-done | bytes 6291472 | tf_op jit(solution)/shard_map/all_gather | solution.py:16
  108.7 5.3 %fusion.9 = f32[1024,512]{1,0:T(8,128)S(1)} fusion(bf16[1024,2048]{1,0:T(8,128)(2,1)} %bitcast.66, bf16[2048,1536]{1,0:T(8,128)(2,1)} %all-gather.3.cloned.1.call-done), kind=kOutput, calls=%fused_computation.14 | convolution fusion | flops 2147483648 | bytes 8388608 | tf_op jit(solution)/shard_map/dot_general | solution.py:90
  114.0 0.6 copy-done.2
  114.6 3.9 %multiply_convert_fusion = (bf16[1024,512]{1,0:T(8,128)(2,1)S(1)}, f32[1024,512]{1,0:T(8,128)}) fusion(f32[1024,512]{1,0:T(8,128)S(1)} %fusion.9, bf16[1024,2048]{1,0:T(8,128)(2,1)S(1)} %bitcast.67, bf16[2048,1536]{1,0:T(8,128)(2,1)S(1)} %copy-done.2), kind=kOutput, calls=%fused_computation.6 | convolution fusion | flops 2150629376 | bytes 11534336 | tf_op jit(solution)/shard_map/dot_general | solution.py:91
  118.5 4.4 %convolution_convert_fusion = bf16[2048,2,512]{2,0,1:T(8,128)(2,1)} fusion(bf16[2,512,512]{2,1,0:T(8,128)(2,1)S(1)} %bitcast.75, bf16[2048,1536]{1,0:T(8,128)(2,1)S(1)} %copy-done.2), kind=kOutput, calls=%fused_computation.3 | convolution fusion | flops 2149580800 | bytes 7340032 | tf_op jit(solution)/shard_map/utx,ix->tui/dot_general | solution.py:95
  122.9 6.3 %copy.39 = bf16[512,4096]{1,0:T(8,128)(2,1)} copy(bf16[512,4096]{0,1:T(8,128)(2,1)} %bitcast.68) | data formatting | bytes 8388608 | tf_op jit(solution)/shard_map/convert_element_type | solution.py:99
  129.3 0.6 copy-done.11
  129.9 36.9 %reduce-scatter.5.cloned.1.call-done = bf16[64,4096]{1,0:T(8,128)(2,1)} async-done(((bf16[512,4096]{1,0:T(8,128)(2,1)}), bf16[64,4096]{1,0:T(8,128)(2,1)}) %reduce-scatter.5.cloned.1.call-update) | async-done | bytes 524304 | tf_op jit(solution)/shard_map/reduce_scatter | solution.py:98
  166.9 2.1 reshape.128
  168.9 1.6 fusion.31
  170.6 0.5 multiply_reduce_fusion
  171.1 0.1 copy.52
  171.1 0.3 fusion.21
  171.4 0.3 fusion.20
  171.7 0.2 broadcast_in_dim.2
  172.0 29.7 %all_to_all.10 = bf16[8,64,2048]{2,1,0:T(8,128)(2,1)S(1)} all-to-all(bf16[8,64,2048]{2,1,0:T(8,128)(2,1)S(1)} %broadcast_in_dim.2), channel_id=1, replica_groups=mesh['fs'=16,'tp'=8] {'tp'}, dimensions={0} | all-to-all | bytes 4194304 | tf_op jit(solution)/shard_map/all_to_all | solution.py:21
  201.6 1.3 fusion.24
  202.9 0.3 copy-done.13
  203.2 0.6 copy-done.14
  203.8 3.3 %multiply_convert_fusion.1 = (bf16[512,512]{1,0:T(8,128)(2,1)S(1)}, bf16[512,512]{1,0:T(8,128)(2,1)S(1)}) fusion(f32[1024,512]{1,0:T(8,128)S(1)} %copy-done.13, f32[1024,512]{1,0:T(8,128)S(1)} %copy-done.14, bf16[512,2048]{1,0:T(8,128)(2,1)S(1)} %bitcast.65, bf16[2048,1536]{1,0:T(8,128)(2,1)} %all-gather.3.cloned.1.call-done), kind=kOutput, calls=%fused_computation.23 | convolution fusion | flops 1077149696 | bytes 7340032 | tf_op jit(solution)/shard_map/dot_general | solution.py:122
  207.1 1.3 fusion.2
  208.4 1.3 fusion.3
  209.8 3.8 %fusion = bf16[2048,1536]{0,1:T(8,128)(2,1)} fusion(f32[2048,512]{0,1:T(8,128)S(1)} %fusion.24, f32[2048,512]{0,1:T(8,128)S(1)} %fusion.2, f32[2048,512]{0,1:T(8,128)S(1)} %fusion.3), kind=kLoop, calls=%fused_computation.1 | loop fusion | flops 12582912 | bytes 18874368 | tf_op jit(solution)/shard_map/convert_element_type | solution.py:157
  213.6 8.6 %copy.48 = bf16[2048,1536]{1,0:T(8,128)(2,1)} copy(bf16[2048,1536]{0,1:T(8,128)(2,1)} %fusion) | data formatting | bytes 12582912
  222.3 2.9 fusion.7
  225.1 4.2 %add_convert_fusion = bf16[512,2048]{1,0:T(8,128)(2,1)} fusion(f32[512,2048]{1,0:T(8,128)S(1)} %fusion.7, bf16[512,512]{1,0:T(8,128)(2,1)S(1)} %get-tuple-element.25, bf16[2048,1536]{1,0:T(8,128)(2,1)} %all-gather.3.cloned.1.call-done), kind=kOutput, calls=%fused_computation.2 | convolution fusion | flops 1075838976 | bytes 8912896 | tf_op jit(solution)/shard_map/dot_general | solution.py:50
  229.4 3.8 %all-to-all-start.1 = ((bf16[8,64,2048]{2,1,0:T(8,128)(2,1)}), bf16[8,64,2048]{2,1,0:T(8,128)(2,1)S(1)}, u32[]{:S(2)}, u32[]{:S(2)}) async-start(bf16[8,64,2048]{2,1,0:T(8,128)(2,1)} %bitcast.14), calls=%async_computation.2 | async-start | bytes 4194304 | tf_op jit(solution)/shard_map/all_to_all | solution.py:45
  233.1 0.8 copy.44
  234.0 0.8 copy.43
  234.8 0.8 copy.42
  235.7 1.1 maximum_convert_fusion
  236.8 23.5 %all-to-all-done.1 = bf16[8,64,2048]{2,1,0:T(8,128)(2,1)S(1)} async-done(((bf16[8,64,2048]{2,1,0:T(8,128)(2,1)}), bf16[8,64,2048]{2,1,0:T(8,128)(2,1)S(1)}, u32[]{:S(2)}, u32[]{:S(2)}) %all-to-all-start.1) | async-done | bytes 2097184 | tf_op jit(solution)/shard_map/all_to_all | solution.py:45
  260.2 1.1 reduce_sum.51
  261.3 1.2 multiply_reduce_fusion.2
  262.6 2.2 fusion.23
  264.8 39.1 %reduce-scatter.7.cloned.1.call-done = bf16[128,1536]{1,0:T(8,128)(2,1)} async-done(((bf16[2048,1536]{1,0:T(8,128)(2,1)}), bf16[128,1536]{1,0:T(8,128)(2,1)}) %reduce-scatter.7.cloned.1.call-update) | async-done | bytes 393232
  303.8 1.2 copy.49
  305.1 0.1 convert_element_type.69
  305.2 0.1 slice_add_fusion
  305.2 0.8 copy.45
  306.1 0.8 copy.46
  306.9 0.8 copy.47
  (40 shorter events, 0.2 us)
Async XLA Ops:
  7.2 38.0 %all-gather.5.cloned.1.call-start = ((), (), s32[]{:S(2)}) async-start(), calls=%async_computation.5 | async-start | bytes 4718592 | tf_op jit(solution)/shard_map/all_gather | solution.py:85
  10.5 98.2 %all-gather.3.cloned.1.call-start = ((), (), s32[]{:S(2)}) async-start(), calls=%async_computation.4 | async-start | bytes 6684672 | tf_op jit(solution)/shard_map/all_gather | solution.py:16
  12.4 154.5 %reduce-scatter.5.cloned.1.call-start = ((), (), s32[]{:S(2)}) async-start(), calls=%async_computation.6 | async-start | bytes 4718592 | tf_op jit(solution)/shard_map/reduce_scatter | solution.py:98
  108.7 5.3 %copy-start = (bf16[2,512,2048]{2,1,0:T(8,128)(2,1)S(1)}, bf16[2,512,2048]{2,1,0:T(8,128)(2,1)}, u32[]{:S(2)}) copy-start(bf16[2,512,2048]{2,1,0:T(8,128)(2,1)} %all-gather.5.cloned.1.call-done) | copy-start | bytes 12582916
  108.7 5.9 %copy-start.2 = (bf16[2048,1536]{1,0:T(8,128)(2,1)S(1)}, bf16[2048,1536]{1,0:T(8,128)(2,1)}, u32[]{:S(2)}) copy-start(bf16[2048,1536]{1,0:T(8,128)(2,1)} %all-gather.3.cloned.1.call-done) | copy-start | bytes 18874372
  114.6 3.9 %copy-start.12 = (f32[1024,512]{1,0:T(8,128)}, f32[1024,512]{1,0:T(8,128)S(1)}, u32[]{:S(2)}) copy-start(f32[1024,512]{1,0:T(8,128)S(1)} %fusion.9) | copy-start | bytes 6291460
  129.2 0.7 copy-start.11
  129.2 41.9 %copy-start.3 = (bf16[64,2048]{1,0:T(8,128)(2,1)S(1)}, bf16[64,2048]{1,0:T(8,128)(2,1)}, u32[]{:S(2)}) copy-start(bf16[64,2048]{1,0:T(8,128)(2,1)} %param.13) | copy-start | bytes 786436
  129.3 174.6 %reduce-scatter.7.cloned.1.call-start = ((), (), s32[]{:S(2)}) async-start(), calls=%async_computation.7 | async-start | bytes 6684672
  201.6 1.6 copy-start.13
  201.6 2.2 copy-start.14
  203.8 3.3 %copy-start.1 = (bf16[2,512,2048]{2,1,0:T(8,128)(2,1)S(1)}, bf16[2,512,2048]{2,1,0:T(8,128)(2,1)}, u32[]{:S(2)}) copy-start(bf16[2,512,2048]{2,1,0:T(8,128)(2,1)} %all-gather.5.cloned.1.call-done) | copy-start | bytes 12582916
  229.4 3.8 %copy-start.7 = (f32[128,512]{1,0:T(8,128)S(1)}, f32[128,512]{1,0:T(8,128)}, u32[]{:S(2)}) copy-start(f32[128,512]{1,0:T(8,128)} %param.21) | copy-start | bytes 786436
  229.4 4.6 %copy-start.8 = (f32[128,512]{1,0:T(8,128)S(1)}, f32[128,512]{1,0:T(8,128)}, u32[]{:S(2)}) copy-start(f32[128,512]{1,0:T(8,128)} %param.20) | copy-start | bytes 786436
  229.4 5.5 %copy-start.9 = (f32[128,512]{1,0:T(8,128)S(1)}, f32[128,512]{1,0:T(8,128)}, u32[]{:S(2)}) copy-start(f32[128,512]{1,0:T(8,128)} %param.19) | copy-start | bytes 786436
  229.4 32.0 %copy-start.10 = (f32[2048]{0:T(1024)S(1)}, f32[2048]{0:T(1024)}, u32[]{:S(2)}) copy-start(f32[2048]{0:T(1024)} %param.14) | copy-start | bytes 24580
  229.4 30.9 %all-to-all-start.1 = ((bf16[8,64,2048]{2,1,0:T(8,128)(2,1)}), bf16[8,64,2048]{2,1,0:T(8,128)(2,1)S(1)}, u32[]{:S(2)}, u32[]{:S(2)}) async-start(bf16[8,64,2048]{2,1,0:T(8,128)(2,1)} %bitcast.14), calls=%async_computation.2 | async-start | bytes 4194304 | tf_op jit(solution)/shard_map/all_to_all | solution.py:45
  261.3 43.8 %copy-start.4 = (f32[128,512]{0,1:T(8,128)S(1)}, f32[128,512]{0,1:T(8,128)}, u32[]{:S(2)}) copy-start(f32[128,512]{0,1:T(8,128)} %copy.44) | copy-start | bytes 786436
  261.3 43.8 %copy-start.5 = (f32[128,512]{0,1:T(8,128)S(1)}, f32[128,512]{0,1:T(8,128)}, u32[]{:S(2)}) copy-start(f32[128,512]{0,1:T(8,128)} %copy.43) | copy-start | bytes 786436
  261.3 43.8 %copy-start.6 = (f32[128,512]{0,1:T(8,128)S(1)}, f32[128,512]{0,1:T(8,128)}, u32[]{:S(2)}) copy-start(f32[128,512]{0,1:T(8,128)} %copy.42) | copy-start | bytes 786436
Sparse Core Ops, SparseCore 0:
  10.6 34.4 all-gather.4
  47.3 61.3 all-gather.2
  129.4 37.4 reduce-scatter.4
  222.4 81.4 reduce-scatter.6
where the time goes:
time: 315 us; the launch traced here: 314 us
  waiting for transfers between devices  196 us (62%)
  blocking collectives  29.7 us (9%)
  matrix products  27.9 us (9%)
  local copies, waits for them, and re-layouts  27.4 us (9%)
  other arithmetic  15.7 us (5%)
  between operations  13.9 us (4%)
  starting transfers between devices  3.91 us (1%)
    all_gather x1, waiting for transfers between devices, sent_together(): lax.all_gather(both, axis, axis=dim, tiled=True)  63.5 us
    unnamed x5, waiting for transfers between devices  39.1 us
    reduce_scatter x1, waiting for transfers between devices, per_device(): lax.psum_scatter(gated_product.reshape(lax.axis_size('tp') * tok_rows, 2...  36.9 us
    all_gather x1, waiting for transfers between devices, per_device(): normed_rows = lax.all_gather(normed, 'tp', axis=1, tiled=True)  32.7 us
    all_to_all x1, blocking collectives, sent_to_all(): lax.all_to_all(jnp.broadcast_to(shard[None], (peers, *shard.shape)), axis...  29.7 us
    all_to_all x1, waiting for transfers between devices, summed_on_arrival(): lax.all_to_all(parts, axis, split_axis=0, concat_axis=0, tiled=True)  23.5 us
    unnamed x39, local copies, waits for them, and re-layouts  17.1 us
    dot_general x2, matrix products, contract_last(): lax.dot_general(first_op, second_op, (((1,), (1,)), ((), ())), preferred_...  7.09 us
  transfers between devices with their start and end apart: 5, of which 5 were waited for; matrix products, arithmetic and copies ran while one was open for 5% of the time, Pallas kernels for 0%

commit v1 on v0

--- a/solution.py
+++ b/solution.py
@@ -82,7 +82,15 @@
     input_rows = jnp.stack([late_input, early_input]).astype(jnp.float32)
     input_inverse = inverse_rms(input_rows)
     normed = (input_rows * input_inverse * pre_gain).astype(jnp.bfloat16)
-    normed_rows = lax.all_gather(normed, "tp", axis=1, tiled=True)
+
+    def teams_trace(original, axis_tag):
+        base_arr = jax.lax.psum(1, axis_name=axis_tag)
+        right_arr = jnp.stack([original] * base_arr)
+        r_now = jax.lax.all_to_all(right_arr, axis_name=axis_tag, split_axis=0, concat_axis=0)
+        finding = jnp.concatenate(r_now, axis=1)
+        return finding
+
+    normed_rows = teams_trace(normed, "tp")
     gate_all, up_all, down_gradient_rows = sent_together(
         (gate_weight, up_weight, down_weight), "fs", 0, 1
     )

time: 315 us -> 285 us (0.905)
  waiting for transfers between devices: 196 us -> 130 us
  blocking collectives: 29.7 us -> 53.9 us
  local copies, waits for them, and re-layouts: 27.4 us -> 32.5 us
  starting transfers between devices: 3.91 us -> 8.42 us
    all_gather x1, waiting for transfers between devices: 63.5 us -> 5.64 us  [sent_together(): lax.all_gather(both, axis, axis=dim, tiled=True)]
    all_gather x1 -> x0, waiting for transfers between devices: 32.7 us -> none  [per_device(): normed_rows = lax.all_gather(normed, 'tp', axis=1, tiled=True)]
    all_to_all x0 -> x1, waiting for transfers between devices: none -> 25.2 us  [sent_to_all(): lax.all_to_all(jnp.broadcast_to(shard[None], (peers, *shard.shape)), axis...]
    all_to_all x1, blocking collectives: 29.7 us -> 53.9 us  [teams_trace(): jax.lax.all_to_all(right_arr, axis_name=axis_tag, split_axis=0, concat_ax...]
    all_to_all x0 -> x1, starting transfers between devices: none -> 4.37 us  [sent_to_all(): lax.all_to_all(jnp.broadcast_to(shard[None], (peers, *shard.shape)), axis...]
    unnamed x5 -> x4, waiting for transfers between devices: 39.1 us -> 38.7 us
  transfers between devices with their start and end apart: 5 -> 5, of which waited for: 5 -> 5; matrix products, arithmetic and copies ran while one was open for 5% -> 8% of each run, Pallas kernels for 0% -> 0%
where the time goes in v1:
time: 285 us; the launch traced here: 284 us
  waiting for transfers between devices  130 us (46%)
  blocking collectives  53.9 us (19%)
  local copies, waits for them, and re-layouts  32.5 us (11%)
  matrix products  30.1 us (11%)
  other arithmetic  15 us (5%)
  between operations  14 us (5%)
  starting transfers between devices  8.42 us (3%)
    all_to_all x1, blocking collectives, teams_trace(): jax.lax.all_to_all(right_arr, axis_name=axis_tag, split_axis=0, concat_ax...  53.9 us
    unnamed x4, waiting for transfers between devices  38.7 us
    reduce_scatter x1, waiting for transfers between devices, per_device(): lax.psum_scatter(gated_product.reshape(lax.axis_size('tp') * tok_rows, 2...  37 us
    all_to_all x1, waiting for transfers between devices, sent_to_all(): lax.all_to_all(jnp.broadcast_to(shard[None], (peers, *shard.shape)), axis...  25.2 us
    all_to_all x1, waiting for transfers between devices, summed_on_arrival(): lax.all_to_all(parts, axis, split_axis=0, concat_axis=0, tiled=True)  23.4 us
    unnamed x39, local copies, waits for them, and re-layouts  16.3 us
    dot_general x2, matrix products, contract_last(): lax.dot_general(first_op, second_op, (((1,), (1,)), ((), ())), preferred_...  7.07 us
    convert_element_type x1, local copies, waits for them, and re-layouts, per_device(): gated_product.reshape(lax.axis_size('tp') * tok_rows, 2 * model_width)  6.37 us
  transfers between devices with their start and end apart: 5, of which 5 were waited for; matrix products, arithmetic and copies ran while one was open for 8% of the time, Pallas kernels for 0%

profile of v1, /device:TPU:0, one launch (start us, length us, event | category | flops | bytes accessed | tf_op | source)
XLA Modules:
  0.0 283.9 jit_solution(8770034890864666315)
XLA Ops:
  7.2 1.8 pad_maximum_fusion
  9.1 1.2 multiply_reduce_fusion.1
  10.4 1.2 multiply_convert_fusion.2
  11.6 0.5 stack.11
  12.1 53.9 %all_to_all.15 = bf16[8,2,64,2048]{3,2,1,0:T(8,128)(2,1)S(1)} all-to-all(bf16[8,2,64,2048]{3,2,1,0:T(8,128)(2,1)S(1)} %stack.11), channel_id=1, replica_groups=mesh['fs'=16,'tp'=8] {'tp'}, dimensions={0} | all-to-all | bytes 8388608 | tf_op jit(solution)/shard_map/all_to_all | solution.py:89
  66.0 2.3 copy.66
  68.3 5.6 %all-gather.2.cloned.1.call-done = bf16[2048,1536]{1,0:T(8,128)(2,1)} async-done(((bf16[128,1536]{1,0:T(8,128)(2,1)}), bf16[2048,1536]{1,0:T(8,128)(2,1)}) %all-gather.2.cloned.1.call-update) | async-done | bytes 6291472 | tf_op jit(solution)/shard_map/all_gather | solution.py:16
  74.0 5.3 %fusion.7 = f32[1024,512]{1,0:T(8,128)S(1)} fusion(bf16[1024,2048]{1,0:T(8,128)(2,1)} %bitcast.69, bf16[2048,1536]{1,0:T(8,128)(2,1)} %all-gather.2.cloned.1.call-done), kind=kOutput, calls=%fused_computation.11 | convolution fusion | flops 2147483648 | bytes 8388608 | tf_op jit(solution)/shard_map/dot_general | solution.py:98
  79.3 0.6 copy-done.1
  79.9 3.9 %multiply_convert_fusion = (bf16[1024,512]{1,0:T(8,128)(2,1)S(1)}, f32[1024,512]{1,0:T(8,128)}) fusion(f32[1024,512]{1,0:T(8,128)S(1)} %fusion.7, bf16[1024,2048]{1,0:T(8,128)(2,1)S(1)} %bitcast.71, bf16[2048,1536]{1,0:T(8,128)(2,1)S(1)} %copy-done.1), kind=kOutput, calls=%fused_computation.5 | convolution fusion | flops 2150629376 | bytes 11534336 | tf_op jit(solution)/shard_map/dot_general | solution.py:99
  83.8 4.4 %convolution_convert_fusion = bf16[2048,2,512]{2,0,1:T(8,128)(2,1)} fusion(bf16[2,512,512]{2,1,0:T(8,128)(2,1)S(1)} %bitcast.79, bf16[2048,1536]{1,0:T(8,128)(2,1)S(1)} %copy-done.1), kind=kOutput, calls=%fused_computation.3 | convolution fusion | flops 2149580800 | bytes 7340032 | tf_op jit(solution)/shard_map/utx,ix->tui/dot_general | solution.py:103
  88.2 6.4 %copy.41 = bf16[512,4096]{1,0:T(8,128)(2,1)} copy(bf16[512,4096]{0,1:T(8,128)(2,1)} %bitcast.72) | data formatting | bytes 8388608 | tf_op jit(solution)/shard_map/convert_element_type | solution.py:107
  94.6 0.7 copy-done.11
  95.3 37.0 %reduce-scatter.5.cloned.1.call-done = bf16[64,4096]{1,0:T(8,128)(2,1)} async-done(((bf16[512,4096]{1,0:T(8,128)(2,1)}), bf16[64,4096]{1,0:T(8,128)(2,1)}) %reduce-scatter.5.cloned.1.call-update) | async-done | bytes 524304 | tf_op jit(solution)/shard_map/reduce_scatter | solution.py:106
  132.3 2.1 reshape.140
  134.3 1.6 fusion.29
  135.9 0.5 multiply_reduce_fusion
  136.4 0.1 copy.54
  136.5 0.3 fusion.19
  136.8 0.3 fusion.18
  137.1 1.6 broadcast_in_dim.2
  138.7 4.4 %all-to-all-start.1 = ((bf16[8,64,2048]{2,1,0:T(8,128)(2,1)}), bf16[8,64,2048]{2,1,0:T(8,128)(2,1)}, u32[]{:S(2)}, u32[]{:S(2)}) async-start(bf16[8,64,2048]{2,1,0:T(8,128)(2,1)} %broadcast_in_dim.2), calls=%async_computation.2 | async-start | bytes 4194304 | tf_op jit(solution)/shard_map/all_to_all | solution.py:21
  143.0 0.2 reduce-scatter.7.cloned.1.call-start
  143.3 1.7 slice.65
  145.0 25.2 %all-to-all-done.1 = bf16[8,64,2048]{2,1,0:T(8,128)(2,1)} async-done(((bf16[8,64,2048]{2,1,0:T(8,128)(2,1)}), bf16[8,64,2048]{2,1,0:T(8,128)(2,1)}, u32[]{:S(2)}, u32[]{:S(2)}) %all-to-all-start.1) | async-done | bytes 2097184 | tf_op jit(solution)/shard_map/all_to_all | solution.py:21
  170.2 3.1 %fusion.22 = f32[2048,512]{0,1:T(8,128)S(1)} fusion(bf16[512,2048]{1,0:T(8,128)(2,1)} %bitcast.15, bf16[1024,512]{1,0:T(8,128)(2,1)} %copy-done.6), kind=kOutput, calls=%fused_computation.34 | convolution fusion | flops 1073741824 | bytes 6815744 | tf_op jit(solution)/shard_map/dot_general | solution.py:56
  173.4 3.8 %multiply_convert_fusion.1 = (bf16[512,512]{1,0:T(8,128)(2,1)S(1)}, bf16[512,512]{1,0:T(8,128)(2,1)S(1)}) fusion(f32[1024,512]{1,0:T(8,128)S(1)} %copy-done.13, f32[1024,512]{1,0:T(8,128)S(1)} %copy-done.14, bf16[512,2048]{1,0:T(8,128)(2,1)} %bitcast.15, bf16[2048,1536]{1,0:T(8,128)(2,1)} %all-gather.2.cloned.1.call-done), kind=kOutput, calls=%fused_computation.20 | convolution fusion | flops 1077149696 | bytes 7340032 | tf_op jit(solution)/shard_map/dot_general | solution.py:130
  177.1 1.3 fusion.31
  178.4 1.3 fusion.30
  179.8 3.9 %fusion = bf16[2048,1536]{0,1:T(8,128)(2,1)} fusion(f32[2048,512]{0,1:T(8,128)S(1)} %fusion.22, f32[2048,512]{0,1:T(8,128)S(1)} %fusion.31, f32[2048,512]{0,1:T(8,128)S(1)} %fusion.30), kind=kLoop, calls=%fused_computation.1 | loop fusion | flops 12582912 | bytes 18874368 | tf_op jit(solution)/shard_map/convert_element_type | solution.py:165
  183.6 8.7 %copy.50 = bf16[2048,1536]{1,0:T(8,128)(2,1)} copy(bf16[2048,1536]{0,1:T(8,128)(2,1)} %fusion) | data formatting | bytes 12582912
  192.3 2.9 %fusion.5 = f32[512,2048]{1,0:T(8,128)S(1)} fusion(bf16[512,512]{1,0:T(8,128)(2,1)S(1)} %get-tuple-element.28, bf16[2048,1536]{1,0:T(8,128)(2,1)} %all-gather.2.cloned.1.call-done), kind=kOutput, calls=%fused_computation.9 | convolution fusion | flops 1073741824 | bytes 6815744 | tf_op jit(solution)/shard_map/dot_general | solution.py:50
  195.2 4.2 %add_convert_fusion = bf16[512,2048]{1,0:T(8,128)(2,1)} fusion(f32[512,2048]{1,0:T(8,128)S(1)} %fusion.5, bf16[512,512]{1,0:T(8,128)(2,1)S(1)} %get-tuple-element.27, bf16[2048,1536]{1,0:T(8,128)(2,1)} %all-gather.2.cloned.1.call-done), kind=kOutput, calls=%fused_computation.2 | convolution fusion | flops 1075838976 | bytes 8912896 | tf_op jit(solution)/shard_map/dot_general | solution.py:50
  199.4 3.8 %all-to-all-start.2 = ((bf16[8,64,2048]{2,1,0:T(8,128)(2,1)}), bf16[8,64,2048]{2,1,0:T(8,128)(2,1)S(1)}, u32[]{:S(2)}, u32[]{:S(2)}) async-start(bf16[8,64,2048]{2,1,0:T(8,128)(2,1)} %bitcast.16), calls=%async_computation.3 | async-start | bytes 4194304 | tf_op jit(solution)/shard_map/all_to_all | solution.py:45
  203.2 0.8 copy.46
  204.0 0.8 copy.45
  204.8 0.8 copy.44
  205.7 1.1 maximum_convert_fusion
  206.8 23.4 %all-to-all-done.2 = bf16[8,64,2048]{2,1,0:T(8,128)(2,1)S(1)} async-done(((bf16[8,64,2048]{2,1,0:T(8,128)(2,1)}), bf16[8,64,2048]{2,1,0:T(8,128)(2,1)S(1)}, u32[]{:S(2)}, u32[]{:S(2)}) %all-to-all-start.2) | async-done | bytes 2097184 | tf_op jit(solution)/shard_map/all_to_all | solution.py:45
  230.2 1.1 reduce_sum.51
  231.4 1.2 multiply_reduce_fusion.2
  232.6 2.2 fusion.21
  234.8 38.7 %reduce-scatter.7.cloned.1.call-done = bf16[128,1536]{1,0:T(8,128)(2,1)} async-done(((bf16[2048,1536]{1,0:T(8,128)(2,1)}), bf16[128,1536]{1,0:T(8,128)(2,1)}) %reduce-scatter.7.cloned.1.call-update) | async-done | bytes 393232
  273.5 1.2 copy.51
  274.8 0.1 slice_add_fusion
  274.9 0.8 copy.47
  275.7 0.8 copy.48
  276.6 0.8 copy.49
  (42 shorter events, 0.3 us)
Async XLA Ops:
  7.2 66.8 %all-gather.2.cloned.1.call-start = ((), (), s32[]{:S(2)}) async-start(), calls=%async_computation.5 | async-start | bytes 6684672 | tf_op jit(solution)/shard_map/all_gather | solution.py:16
  9.1 123.2 %reduce-scatter.5.cloned.1.call-start = ((), (), s32[]{:S(2)}) async-start(), calls=%async_computation.6 | async-start | bytes 4718592 | tf_op jit(solution)/shard_map/reduce_scatter | solution.py:106
  74.0 5.3 %copy-start = (bf16[8,2,64,2048]{3,2,0,1:T(8,128)(2,1)S(1)}, bf16[8,2,64,2048]{3,2,0,1:T(8,128)(2,1)}, u32[]{:S(2)}) copy-start(bf16[8,2,64,2048]{3,2,0,1:T(8,128)(2,1)} %copy.66) | copy-start | bytes 12582916
  74.0 5.9 %copy-start.1 = (bf16[2048,1536]{1,0:T(8,128)(2,1)S(1)}, bf16[2048,1536]{1,0:T(8,128)(2,1)}, u32[]{:S(2)}) copy-start(bf16[2048,1536]{1,0:T(8,128)(2,1)} %all-gather.2.cloned.1.call-done) | copy-start | bytes 18874372
  79.9 3.9 %copy-start.12 = (f32[1024,512]{1,0:T(8,128)}, f32[1024,512]{1,0:T(8,128)S(1)}, u32[]{:S(2)}) copy-start(f32[1024,512]{1,0:T(8,128)S(1)} %fusion.7) | copy-start | bytes 6291460
  83.8 4.4 %copy-start.6 = (bf16[1024,512]{1,0:T(8,128)(2,1)}, bf16[1024,512]{1,0:T(8,128)(2,1)S(1)}, u32[]{:S(2)}) copy-start(bf16[1024,512]{1,0:T(8,128)(2,1)S(1)} %get-tuple-element.38) | copy-start | bytes 3145732
  94.6 0.7 copy-start.11
  94.6 41.9 %copy-start.2 = (bf16[64,2048]{1,0:T(8,128)(2,1)S(1)}, bf16[64,2048]{1,0:T(8,128)(2,1)}, u32[]{:S(2)}) copy-start(bf16[64,2048]{1,0:T(8,128)(2,1)} %param.13) | copy-start | bytes 786436
  138.7 31.5 %all-to-all-start.1 = ((bf16[8,64,2048]{2,1,0:T(8,128)(2,1)}), bf16[8,64,2048]{2,1,0:T(8,128)(2,1)}, u32[]{:S(2)}, u32[]{:S(2)}) async-start(bf16[8,64,2048]{2,1,0:T(8,128)(2,1)} %broadcast_in_dim.2), calls=%async_computation.2 | async-start | bytes 4194304 | tf_op jit(solution)/shard_map/all_to_all | solution.py:21
  143.0 130.4 %reduce-scatter.7.cloned.1.call-start = ((), (), s32[]{:S(2)}) async-start(), calls=%async_computation.7 | async-start | bytes 6684672
  170.2 3.1 %copy-start.13 = (f32[1024,512]{1,0:T(8,128)S(1)}, f32[1024,512]{1,0:T(8,128)}, u32[]{:S(2)}) copy-start(f32[1024,512]{1,0:T(8,128)} %copy-done.12) | copy-start | bytes 6291460
  170.2 3.1 %copy-start.14 = (f32[1024,512]{1,0:T(8,128)S(1)}, f32[1024,512]{1,0:T(8,128)}, u32[]{:S(2)}) copy-start(f32[1024,512]{1,0:T(8,128)} %get-tuple-element.39) | copy-start | bytes 6291460
  199.4 3.8 %copy-start.7 = (f32[128,512]{1,0:T(8,128)S(1)}, f32[128,512]{1,0:T(8,128)}, u32[]{:S(2)}) copy-start(f32[128,512]{1,0:T(8,128)} %param.21) | copy-start | bytes 786436
  199.4 4.6 %copy-start.8 = (f32[128,512]{1,0:T(8,128)S(1)}, f32[128,512]{1,0:T(8,128)}, u32[]{:S(2)}) copy-start(f32[128,512]{1,0:T(8,128)} %param.20) | copy-start | bytes 786436
  199.4 5.5 %copy-start.9 = (f32[128,512]{1,0:T(8,128)S(1)}, f32[128,512]{1,0:T(8,128)}, u32[]{:S(2)}) copy-start(f32[128,512]{1,0:T(8,128)} %param.19) | copy-start | bytes 786436
  199.4 32.0 %copy-start.10 = (f32[2048]{0:T(1024)S(1)}, f32[2048]{0:T(1024)}, u32[]{:S(2)}) copy-start(f32[2048]{0:T(1024)} %param.14) | copy-start | bytes 24580
  199.4 30.9 %all-to-all-start.2 = ((bf16[8,64,2048]{2,1,0:T(8,128)(2,1)}), bf16[8,64,2048]{2,1,0:T(8,128)(2,1)S(1)}, u32[]{:S(2)}, u32[]{:S(2)}) async-start(bf16[8,64,2048]{2,1,0:T(8,128)(2,1)} %bitcast.16), calls=%async_computation.3 | async-start | bytes 4194304 | tf_op jit(solution)/shard_map/all_to_all | solution.py:45
  231.3 43.4 %copy-start.3 = (f32[128,512]{0,1:T(8,128)S(1)}, f32[128,512]{0,1:T(8,128)}, u32[]{:S(2)}) copy-start(f32[128,512]{0,1:T(8,128)} %copy.46) | copy-start | bytes 786436
  231.3 43.4 %copy-start.4 = (f32[128,512]{0,1:T(8,128)S(1)}, f32[128,512]{0,1:T(8,128)}, u32[]{:S(2)}) copy-start(f32[128,512]{0,1:T(8,128)} %copy.45) | copy-start | bytes 786436
  231.4 43.4 %copy-start.5 = (f32[128,512]{0,1:T(8,128)S(1)}, f32[128,512]{0,1:T(8,128)}, u32[]{:S(2)}) copy-start(f32[128,512]{0,1:T(8,128)} %copy.44) | copy-start | bytes 786436
Sparse Core Ops, SparseCore 0:
  10.1 63.8 all-gather.1
  94.7 37.4 reduce-scatter.4
  192.4 81.0 reduce-scatter.6
